TPU v7x, 32 devices: a whole 2x2x4 slice. The times are simulated.
32 devices in a mesh: sp: 16 (over z, y, x), tp: 2 (over core).
Axes of the slice: x: 2, y: 2, z: 4, core: 2. Of those that a mesh axis runs over, the one named last changes fastest.
Arguments:
- tokens: bfloat16 [8192, 2048], P('sp', 'tp'), may hold values from -6 to 6
- input_gain: bfloat16 [2048], P('tp'), may hold values from 0.099609375 to 1.8984375
- query_weight: bfloat16 [2048, 1024], P(None, 'tp'), may hold values from -10 to 10
- key_weight: bfloat16 [2048, 1024], P(None, 'tp'), may hold values from -10 to 10
- value_weight: bfloat16 [2048, 1024], P(None, 'tp'), may hold values from -0.125 to 0.125
- pool_in_weight: bfloat16 [2048, 1024], P(None, 'tp'), may hold values from -0.125 to 0.125
- log_gates: float32 [8, 8192], P('tp'), may hold values from -8192 to 0, as said below
- pool_weight: bfloat16 [8, 128, 128], P('tp'), may hold values from -0.5 to 0.5
- pool_scale: float32 [1024], P('tp'), may hold values from 0.1 to 1.9
- attention_out: bfloat16 [1024, 2048], P('tp'), may hold values from -16 to 16
- pooling_out: bfloat16 [1024, 2048], P('tp'), may hold values from -16 to 16
- final_gain: float32 [2048], P('tp'), may hold values from 0.1 to 1.9
Outputs:
- layer_out: bfloat16 [8192, 2048], P('sp', 'tp')
Inputs may be any that keep to these rules, and one draw needn't show every extreme that they name: `log_gates`: each row does not increase along positions.
All inputs are finite; a program needn't handle non-finite values.
Results may differ from a plain program's by a relative error of at most 0.015.
Values may be sent and summed in bfloat16 or wider, within the bound.
A program may use at most 128 MiB of HBM per device.

v0:
```python
import jax
import jax.numpy as jnp
from jax import lax
from jax.sharding import PartitionSpec as P

WINDOW_MAX = 16
very_low = -1e30
epsilon = 1e-06
key_span = 2048


def passed_along(block, axis, distance):
    devices = range(lax.axis_size(axis))
    route = [(i - distance, i) for i in devices if i - distance in devices]
    return lax.ppermute(block, axis, route)


def attend_block(state, queries, query_gate, query_first, keys, values, key_gate, key_first):
    maxima, totals, summed = state
    head_size = queries.shape[2]
    scores = jnp.einsum(
        "thd,shd->ths", queries, keys, preferred_element_type=jnp.float32
    ) * head_size ** (-0.5)
    scores = scores + query_gate[:, :, None] - key_gate[None, :, :]
    query_rows = query_first + jnp.arange(queries.shape[0], dtype=jnp.int32)
    key_rows = key_first + jnp.arange(keys.shape[0], dtype=jnp.int32)
    allowed = (query_rows[:, None] >= key_rows[None, :])[:, None, :]
    scores = jnp.where(allowed, scores, very_low)
    new_max = jnp.maximum(maxima, jnp.max(scores, axis=2))
    weights = jnp.where(allowed, jnp.exp(scores - new_max[:, :, None]), 0.0)
    factor = jnp.exp(maxima - new_max)
    totals = factor * totals + jnp.sum(weights, axis=2)
    summed = factor[:, :, None] * summed + jnp.einsum(
        "ths,shd->thd", weights.astype(jnp.bfloat16), values, preferred_element_type=jnp.float32
    )
    return (new_max, totals, summed)


def attend(state, queries, query_gate, query_first, keys, values, log_gates):
    count = keys.shape[0]
    heads = queries.shape[1]
    head_size = queries.shape[2]
    span = count
    for halving in range(24):
        if span > key_span and span % 2 == 0:
            span = span // 2
    pieces = count // span
    keys_blocked = keys.reshape(pieces, span, heads, head_size)
    values_blocked = values.reshape(pieces, span, heads, head_size)
    gates_blocked = log_gates.reshape(heads, pieces, span).transpose(1, 0, 2)
    block_starts = span * jnp.arange(pieces, dtype=jnp.int32)

    def step(carry, block):
        return (
            attend_block(
                carry, queries, query_gate, query_first, block[0], block[1], block[2], block[3]
            ),
            None,
        )

    state, unused = lax.scan(
        step, state, (keys_blocked, values_blocked, gates_blocked, block_starts)
    )
    return state


def body(
    tokens,
    input_gain,
    query_weight,
    key_weight,
    value_weight,
    pool_in_weight,
    log_gates,
    pool_weight,
    pool_scale,
    attention_out,
    pooling_out,
    final_gain,
):
    tok_rows = tokens.shape[0]
    width = query_weight.shape[0]
    groups = pool_weight.shape[0]
    head_size = pool_weight.shape[1]
    heads = log_gates.shape[0]
    attention_width = query_weight.shape[1]
    pool_width = pool_in_weight.shape[1]
    sequence_index = lax.axis_index("sp")
    first_row = sequence_index * tok_rows
    last_row = first_row + tok_rows - 1
    part = lax.all_gather(tokens, "tp", axis=1, tiled=True)
    gain_part = lax.all_gather(input_gain.reshape(1, -1), "tp", axis=1, tiled=True)
    widened = part.astype(jnp.float32)
    scaled = (widened * gain_part.astype(jnp.float32)).astype(jnp.bfloat16)

    def product(weight):
        return jnp.dot(scaled, weight, preferred_element_type=jnp.float32)

    inverse = lax.rsqrt(jnp.sum(widened * widened, axis=1) / width + epsilon)[:, None]
    query = (
        (product(query_weight) * inverse).astype(jnp.bfloat16).reshape(tok_rows, heads, head_size)
    )
    keys = (product(key_weight) * inverse).astype(jnp.bfloat16)
    values = (product(value_weight) * inverse).astype(jnp.bfloat16)
    pool_input = (product(pool_in_weight) * inverse).astype(jnp.bfloat16)
    query_gate = lax.dynamic_slice_in_dim(log_gates, first_row, tok_rows, 1).T
    state = (
        jnp.full((tok_rows, heads), very_low, jnp.float32),
        jnp.zeros((tok_rows, heads), jnp.float32),
        jnp.zeros((tok_rows, heads, head_size), jnp.float32),
    )
    carry = state
    pieces = (
        lax.all_gather(keys, "sp", axis=0, tiled=True),
        lax.all_gather(values, "sp", axis=0, tiled=True),
    )
    state = lax.cond(
        jnp.int32(0) > last_row,
        lambda: carry,
        lambda: attend(carry, query, query_gate, first_row, pieces[0], pieces[1], log_gates),
    )
    maxima, totals, summed = state
    attended = (summed / totals[:, :, None]).astype(jnp.bfloat16).reshape(tok_rows, attention_width)
    rim = passed_along(pool_input[tok_rows - (WINDOW_MAX - 1) :], "sp", 1)
    extended = jnp.concatenate([rim, pool_input], axis=0).astype(jnp.float32)
    column = jnp.arange(pool_width, dtype=jnp.int32)
    group_number = lax.axis_index("tp") * groups + column // head_size
    window = jnp.left_shift(jnp.full((pool_width,), 2, jnp.int32), group_number % 4)
    sums = extended
    span = 1
    chosen = jnp.zeros((tok_rows, pool_width), jnp.float32)
    for level in range(4):
        sums = sums[span:] + sums[:-span]
        span = span * 2
        offset_rows = WINDOW_MAX - span
        chosen = jnp.where(
            window[None, :] == span, sums[offset_rows : offset_rows + tok_rows], chosen
        )
    element_locations = first_row + jnp.arange(tok_rows, dtype=jnp.int32)
    counts = jnp.minimum(window[None, :], element_locations[:, None] + 1).astype(jnp.float32)
    departure = (chosen / counts - pool_input.astype(jnp.float32)).astype(jnp.bfloat16)
    mapped = jnp.einsum(
        "tgc,gcd->tgd",
        departure.reshape(tok_rows, groups, head_size),
        pool_weight,
        preferred_element_type=jnp.float32,
    )
    pooled = (mapped.reshape(tok_rows, pool_width) * pool_scale).astype(jnp.bfloat16)
    numbers = (((0,), (1,)), ((), ()))
    mixed = lax.psum_scatter(
        (
            lax.dot_general(attention_out, attended, numbers, preferred_element_type=jnp.float32)
            + lax.dot_general(pooling_out, pooled, numbers, preferred_element_type=jnp.float32)
        ).astype(jnp.bfloat16),
        "tp",
        scatter_dimension=0,
        tiled=True,
    ).astype(jnp.float32)
    squares = lax.psum(jnp.sum(mixed * mixed, axis=0), "tp")
    out_inverse = lax.rsqrt(squares / width + epsilon)
    return (mixed * out_inverse[None, :] * final_gain[:, None]).T.astype(jnp.bfloat16)


def solution(mesh):
    return jax.shard_map(
        body,
        mesh=mesh,
        in_specs=(
            P("sp", "tp"),
            P("tp"),
            P(None, "tp"),
            P(None, "tp"),
            P(None, "tp"),
            P(None, "tp"),
            P("tp", None),
            P("tp", None, None),
            P("tp"),
            P("tp", None),
            P("tp", None),
            P("tp"),
        ),
        out_specs=P("sp", "tp"),
        check_vma=False,
    )
```

profile of v0, /device:TPU:0, one launch (start us, length us, event | category | flops | bytes accessed | tf_op | source)
XLA Modules:
  0.0 463.4 jit_solution(7323547695319961552)
XLA Ops:
  9.4 12.8 %all-gather.5.cloned.1.call-done = bf16[512,2048]{1,0:T(8,128)(2,1)} async-done(((bf16[512,1024]{1,0:T(8,128)(2,1)}), bf16[512,2048]{1,0:T(8,128)(2,1)}) %all-gather.5.cloned.1.call-update) | async-done | bytes 2097168 | tf_op jit(solution)/shard_map/all_gather | solution.py:91
  24.5 3.7 fusion.34
  28.2 4.3 fusion.37
  33.9 3.6 fusion.43
  37.6 3.6 collective-permute-start
  45.9 95.9 %all-gather.7.cloned.1.call-done = bf16[8192,512]{1,0:T(8,128)(2,1)} async-done(((bf16[512,512]{1,0:T(8,128)(2,1)}), bf16[8192,512]{1,0:T(8,128)(2,1)}) %all-gather.7.cloned.1.call-update) | async-done | bytes 8388624 | tf_op jit(solution)/shard_map/all_gather | solution.py:114
  141.8 113.3 %all-gather.9.cloned.1.call-done = bf16[8192,512]{1,0:T(8,128)(2,1)} async-done(((bf16[512,512]{1,0:T(8,128)(2,1)}), bf16[8192,512]{1,0:T(8,128)(2,1)}) %all-gather.9.cloned.1.call-update) | async-done | bytes 8388624 | tf_op jit(solution)/shard_map/all_gather | solution.py:115
  255.0 181.5 %conditional.1 = (f32[512,4]{0,1:T(4,128)S(1)}, f32[512,4,128]{0,2,1:T(8,128)}) conditional(s32[]{:T(128)} %convert_element_type.58, (bf16[8192,512]{1,0:T(8,128)(2,1)}, bf16[8192,512]{1,0:T(8,128)(2,1)}, f32[4,8192]{1,0:T(4,128)}, bf16[512,512]{1,0:T(8,128)(2,1)S(1)}, s32[]{:T(128)}, /*index=5*/f32[512,4]{0,1:T(4,128)}) %tuple.17, () %tuple.18), branch_computations={%region_1.6_spmd, %region_6.7_spmd} | conditional | flops 2229023232 | bytes 112046448 | solution.py:117
  255.0 12.6 %reshape.108 = bf16[4,2048,4,128]{3,2,1,0:T(4,128)(2,1)} reshape(bf16[8192,512]{1,0:T(8,128)(2,1)} %get-tuple-element.75) | data formatting | bytes 16777216 | tf_op jit(solution)/shard_map/cond/branch_0_fun/reshape | solution.py:48
  267.6 12.5 %reshape.111 = bf16[4,2048,4,128]{3,2,1,0:T(4,128)(2,1)} reshape(bf16[8192,512]{1,0:T(8,128)(2,1)} %get-tuple-element.79) | data formatting | bytes 16777216 | tf_op jit(solution)/shard_map/cond/branch_0_fun/reshape | solution.py:49
  281.4 155.2 %while.14 = (s32[]{:T(128)}, f32[512,4]{0,1:T(4,128)S(1)}, f32[512,4]{0,1:T(4,128)S(1)}, f32[512,4,128]{0,2,1:T(8,128)}, s32[]{:T(128)}, /*index=5*/s32[4]{0:T(1...) while((s32[]{:T(128)}, f32[512,4]{0,1:T(4,128)S(1)}, ...), condition=%wide.region_5.5_spmd.clone, body=%wide.region_2.4_spmd.clone.sunk | while | flops 2229023232 | bytes 76361920 | solution.py:61
  283.6 4.1 constant_dynamic-slice_fusion.3
  288.4 7.7 %fusion.87 = (f32[512,4]{0,1:T(4,128)S(1)}, f32[4,2048,512]{2,1,0:T(8,128)}) fusion(f32[4,2048]{1,0:T(4,128)S(1)} %dynamic-slice_bitcast_fusion.3, f32[512,4]{0,1:T(4,128)S(1)} %get-tuple-element.303, pred[512,2048]{0,1:T(8,128)(4,1)S(1)} %broadcast_compare_fusion.6, bf16[512,4,128]{2,0,1:T(8,128)(2,1)S(1)} %copy-done.5, ...), kind=kOutput, calls=%fused_computation.6.clone.1 | convolution fusion | flops 1094711296 | bytes 20496384 | tf_op jit(solution)/shard_map/cond/branch_0_fun/while/body/eval_jaxpr/thd,shd->ths/dot_general | solution.py:21
  296.1 8.8 %fusion.88 = f32[512,4]{0,1:T(4,128)S(1)} fusion(f32[4,2048,512]{2,1,0:T(8,128)} %get-tuple-element.265, f32[512,4]{0,1:T(4,128)S(1)} %select_maximum_fusion.2, f32[4,2048]{1,0:T(4,128)S(1)} %dynamic-slice_bitcast_fusion.3, f32[512,4]{0,1:T(4,128)S(1)} %get-tuple-element.303, pred[512,2048]{0,1:T(8,128)(4,1)S(1)} %broadcast_compare_fusion.6), kind=kLoop, calls=%fused_computation.5.clone.1 | loop fusion | flops 29358080 | bytes 17883136 | tf_op jit(solution)/shard_map/cond/branch_0_fun/while/body/eval_jaxpr/reduce_sum | solution.py:32
  304.9 4.4 copy.46
  309.3 10.8 %fusion.90 = f32[512,4,128]{0,2,1:T(8,128)} fusion(f32[4,2048,512]{2,1,0:T(8,128)} %get-tuple-element.265, f32[512,4]{0,1:T(4,128)S(1)} %select_maximum_fusion.2, f32[4,2048]{1,0:T(4,128)S(1)} %dynamic-slice_bitcast_fusion.3, f32[512,4]{0,1:T(4,128)S(1)} %get-tuple-element.303, pred[512,2048]{0,1:T(8,128)(4,1)S(1)} %broadcast_compare_fusion.6, ...), kind=kOutput, calls=%fused_computation.14.clone.1 | convolution fusion | flops 1103888384 | bytes 22077440 | tf_op jit(solution)/shard_map/cond/branch_0_fun/while/body/eval_jaxpr/ths,shd->thd/dot_general | solution.py:33
  322.2 4.1 constant_dynamic-slice_fusion.3
  327.0 7.7 %fusion.87 = (f32[512,4]{0,1:T(4,128)S(1)}, f32[4,2048,512]{2,1,0:T(8,128)}) fusion(f32[4,2048]{1,0:T(4,128)S(1)} %dynamic-slice_bitcast_fusion.3, f32[512,4]{0,1:T(4,128)S(1)} %get-tuple-element.303, pred[512,2048]{0,1:T(8,128)(4,1)S(1)} %broadcast_compare_fusion.6, bf16[512,4,128]{2,0,1:T(8,128)(2,1)S(1)} %copy-done.5, ...), kind=kOutput, calls=%fused_computation.6.clone.1 | convolution fusion | flops 1094711296 | bytes 20496384 | tf_op jit(solution)/shard_map/cond/branch_0_fun/while/body/eval_jaxpr/thd,shd->ths/dot_general | solution.py:21
  334.7 8.8 %fusion.88 = f32[512,4]{0,1:T(4,128)S(1)} fusion(f32[4,2048,512]{2,1,0:T(8,128)} %get-tuple-element.265, f32[512,4]{0,1:T(4,128)S(1)} %select_maximum_fusion.2, f32[4,2048]{1,0:T(4,128)S(1)} %dynamic-slice_bitcast_fusion.3, f32[512,4]{0,1:T(4,128)S(1)} %get-tuple-element.303, pred[512,2048]{0,1:T(8,128)(4,1)S(1)} %broadcast_compare_fusion.6), kind=kLoop, calls=%fused_computation.5.clone.1 | loop fusion | flops 29358080 | bytes 17883136 | tf_op jit(solution)/shard_map/cond/branch_0_fun/while/body/eval_jaxpr/reduce_sum | solution.py:32
  343.5 4.4 copy.46
  347.9 11.0 %fusion.90 = f32[512,4,128]{0,2,1:T(8,128)} fusion(f32[4,2048,512]{2,1,0:T(8,128)} %get-tuple-element.265, f32[512,4]{0,1:T(4,128)S(1)} %select_maximum_fusion.2, f32[4,2048]{1,0:T(4,128)S(1)} %dynamic-slice_bitcast_fusion.3, f32[512,4]{0,1:T(4,128)S(1)} %get-tuple-element.303, pred[512,2048]{0,1:T(8,128)(4,1)S(1)} %broadcast_compare_fusion.6, ...), kind=kOutput, calls=%fused_computation.14.clone.1 | convolution fusion | flops 1103888384 | bytes 22077440 | tf_op jit(solution)/shard_map/cond/branch_0_fun/while/body/eval_jaxpr/ths,shd->thd/dot_general | solution.py:33
  361.1 4.1 constant_dynamic-slice_fusion.3
  365.9 7.6 %fusion.87 = (f32[512,4]{0,1:T(4,128)S(1)}, f32[4,2048,512]{2,1,0:T(8,128)}) fusion(f32[4,2048]{1,0:T(4,128)S(1)} %dynamic-slice_bitcast_fusion.3, f32[512,4]{0,1:T(4,128)S(1)} %get-tuple-element.303, pred[512,2048]{0,1:T(8,128)(4,1)S(1)} %broadcast_compare_fusion.6, bf16[512,4,128]{2,0,1:T(8,128)(2,1)S(1)} %copy-done.5, ...), kind=kOutput, calls=%fused_computation.6.clone.1 | convolution fusion | flops 1094711296 | bytes 20496384 | tf_op jit(solution)/shard_map/cond/branch_0_fun/while/body/eval_jaxpr/thd,shd->ths/dot_general | solution.py:21
  373.5 8.8 %fusion.88 = f32[512,4]{0,1:T(4,128)S(1)} fusion(f32[4,2048,512]{2,1,0:T(8,128)} %get-tuple-element.265, f32[512,4]{0,1:T(4,128)S(1)} %select_maximum_fusion.2, f32[4,2048]{1,0:T(4,128)S(1)} %dynamic-slice_bitcast_fusion.3, f32[512,4]{0,1:T(4,128)S(1)} %get-tuple-element.303, pred[512,2048]{0,1:T(8,128)(4,1)S(1)} %broadcast_compare_fusion.6), kind=kLoop, calls=%fused_computation.5.clone.1 | loop fusion | flops 29358080 | bytes 17883136 | tf_op jit(solution)/shard_map/cond/branch_0_fun/while/body/eval_jaxpr/reduce_sum | solution.py:32
  382.3 4.4 copy.46
  386.8 11.0 %fusion.90 = f32[512,4,128]{0,2,1:T(8,128)} fusion(f32[4,2048,512]{2,1,0:T(8,128)} %get-tuple-element.265, f32[512,4]{0,1:T(4,128)S(1)} %select_maximum_fusion.2, f32[4,2048]{1,0:T(4,128)S(1)} %dynamic-slice_bitcast_fusion.3, f32[512,4]{0,1:T(4,128)S(1)} %get-tuple-element.303, pred[512,2048]{0,1:T(8,128)(4,1)S(1)} %broadcast_compare_fusion.6, ...), kind=kOutput, calls=%fused_computation.14.clone.1 | convolution fusion | flops 1103888384 | bytes 22077440 | tf_op jit(solution)/shard_map/cond/branch_0_fun/while/body/eval_jaxpr/ths,shd->thd/dot_general | solution.py:33
  399.9 4.1 constant_dynamic-slice_fusion.3
  404.7 7.6 %fusion.87 = (f32[512,4]{0,1:T(4,128)S(1)}, f32[4,2048,512]{2,1,0:T(8,128)}) fusion(f32[4,2048]{1,0:T(4,128)S(1)} %dynamic-slice_bitcast_fusion.3, f32[512,4]{0,1:T(4,128)S(1)} %get-tuple-element.303, pred[512,2048]{0,1:T(8,128)(4,1)S(1)} %broadcast_compare_fusion.6, bf16[512,4,128]{2,0,1:T(8,128)(2,1)S(1)} %copy-done.5, ...), kind=kOutput, calls=%fused_computation.6.clone.1 | convolution fusion | flops 1094711296 | bytes 20496384 | tf_op jit(solution)/shard_map/cond/branch_0_fun/while/body/eval_jaxpr/thd,shd->ths/dot_general | solution.py:21
  412.4 8.8 %fusion.88 = f32[512,4]{0,1:T(4,128)S(1)} fusion(f32[4,2048,512]{2,1,0:T(8,128)} %get-tuple-element.265, f32[512,4]{0,1:T(4,128)S(1)} %select_maximum_fusion.2, f32[4,2048]{1,0:T(4,128)S(1)} %dynamic-slice_bitcast_fusion.3, f32[512,4]{0,1:T(4,128)S(1)} %get-tuple-element.303, pred[512,2048]{0,1:T(8,128)(4,1)S(1)} %broadcast_compare_fusion.6), kind=kLoop, calls=%fused_computation.5.clone.1 | loop fusion | flops 29358080 | bytes 17883136 | tf_op jit(solution)/shard_map/cond/branch_0_fun/while/body/eval_jaxpr/reduce_sum | solution.py:32
  421.2 4.4 copy.46
  425.6 11.0 %fusion.90 = f32[512,4,128]{0,2,1:T(8,128)} fusion(f32[4,2048,512]{2,1,0:T(8,128)} %get-tuple-element.265, f32[512,4]{0,1:T(4,128)S(1)} %select_maximum_fusion.2, f32[4,2048]{1,0:T(4,128)S(1)} %dynamic-slice_bitcast_fusion.3, f32[512,4]{0,1:T(4,128)S(1)} %get-tuple-element.303, pred[512,2048]{0,1:T(8,128)(4,1)S(1)} %broadcast_compare_fusion.6, ...), kind=kOutput, calls=%fused_computation.14.clone.1 | convolution fusion | flops 1103888384 | bytes 22077440 | tf_op jit(solution)/shard_map/cond/branch_0_fun/while/body/eval_jaxpr/ths,shd->thd/dot_general | solution.py:33
  442.5 7.9 %reduce-scatter.2.cloned.1.call-done = bf16[1024,512]{0,1:T(8,128)(2,1)} async-done(((bf16[2048,512]{0,1:T(8,128)(2,1)}), bf16[1024,512]{0,1:T(8,128)(2,1)}) %reduce-scatter.2.cloned.1.call-update) | async-done | bytes 1048592 | tf_op jit(solution)/shard_map/reduce_scatter | solution.py:150
  (98 shorter events, 36.4 us)
Async XLA Ops:
  6.5 431.4 %copy-start = (bf16[512,2048]{1,0:T(8,128)(2,1)S(1)}, bf16[512,2048]{1,0:T(8,128)(2,1)}, u32[]{:S(2)}) copy-start(bf16[512,2048]{1,0:T(8,128)(2,1)} %param.25) | copy-start | bytes 6291460
  6.5 15.7 %all-gather.5.cloned.1.call-start = ((), (), s32[]{:S(2)}) async-start(), calls=%async_computation.1 | async-start | bytes 3145728 | tf_op jit(solution)/shard_map/all_gather | solution.py:91
  7.3 134.5 %all-gather.7.cloned.1.call-start = ((), (), s32[]{:S(2)}) async-start(), calls=%async_computation.2 | async-start | bytes 8912896 | tf_op jit(solution)/shard_map/all_gather | solution.py:114
  22.2 2.2 copy-start.2
  28.1 226.9 %all-gather.9.cloned.1.call-start = ((), (), s32[]{:S(2)}) async-start(), calls=%async_computation.3 | async-start | bytes 8912896 | tf_op jit(solution)/shard_map/all_gather | solution.py:115
  32.5 417.9 %reduce-scatter.2.cloned.1.call-start = ((), (), s32[]{:S(2)}) async-start(), calls=%async_computation.4 | async-start | bytes 3145728 | tf_op jit(solution)/shard_map/reduce_scatter | solution.py:150
  33.9 7.3 %copy-start.3 = (bf16[512,2048]{1,0:T(8,128)(2,1)S(1)}, bf16[512,2048]{1,0:T(8,128)(2,1)}, u32[]{:S(2)}) copy-start(bf16[512,2048]{1,0:T(8,128)(2,1)} %all-gather.5.cloned.1.call-done) | copy-start | bytes 6291460
  33.9 7.3 %copy-start.9 = (bf16[2048,512]{1,0:T(8,128)(2,1)S(1)}, bf16[2048,512]{1,0:T(8,128)(2,1)}, u32[]{:S(2)}) copy-start(bf16[2048,512]{1,0:T(8,128)(2,1)} %param.18) | copy-start | bytes 6291460
  37.6 5.2 %collective-permute-start = (bf16[15,512]{1,0:T(8,128)(2,1)S(1)}, bf16[15,512]{1,0:T(8,128)(2,1)S(1)}, u32[]{:S(2)}, u32[]{:S(2)}) collective-permute-start(bf16[15,512]{1,0:T(8,128)(2,1)S(1)} %slice.45), channel_id=1, source_target_pairs={{0,2},{2,4},{4,6},{6,8},{8,10},{10,12},{12,14},{14,16},{16,18},{18... | collective-permute-start | bytes 46088 | tf_op jit(solution)/shard_map/ppermute | solution.py:15
  43.2 0.9 copy-start.10
  44.1 0.9 copy-start.8
  280.1 1.3 copy-start.6
  283.6 4.8 %copy-start.5 = (bf16[512,4,128]{2,0,1:T(8,128)(2,1)S(1)}, bf16[512,4,128]{2,0,1:T(8,128)(2,1)}, u32[]{:S(2)}) copy-start(bf16[512,4,128]{2,0,1:T(8,128)(2,1)} %get-tuple-element.302) | copy-start | bytes 1572868 | tf_op jit(solution)/shard_map/cond/branch_0_fun/while
  322.2 4.8 %copy-start.5 = (bf16[512,4,128]{2,0,1:T(8,128)(2,1)S(1)}, bf16[512,4,128]{2,0,1:T(8,128)(2,1)}, u32[]{:S(2)}) copy-start(bf16[512,4,128]{2,0,1:T(8,128)(2,1)} %get-tuple-element.302) | copy-start | bytes 1572868 | tf_op jit(solution)/shard_map/cond/branch_0_fun/while
  361.0 4.8 %copy-start.5 = (bf16[512,4,128]{2,0,1:T(8,128)(2,1)S(1)}, bf16[512,4,128]{2,0,1:T(8,128)(2,1)}, u32[]{:S(2)}) copy-start(bf16[512,4,128]{2,0,1:T(8,128)(2,1)} %get-tuple-element.302) | copy-start | bytes 1572868 | tf_op jit(solution)/shard_map/cond/branch_0_fun/while
  399.9 4.8 %copy-start.5 = (bf16[512,4,128]{2,0,1:T(8,128)(2,1)S(1)}, bf16[512,4,128]{2,0,1:T(8,128)(2,1)}, u32[]{:S(2)}) copy-start(bf16[512,4,128]{2,0,1:T(8,128)(2,1)} %get-tuple-element.302) | copy-start | bytes 1572868 | tf_op jit(solution)/shard_map/cond/branch_0_fun/while
  438.0 1.3 copy-start.1
  438.0 1.8 copy-start.4
  442.4 11.9 %copy-start.7 = (f32[1024]{0:T(1024)S(1)}, f32[1024]{0:T(1024)}, u32[]{:S(2)}) copy-start(f32[1024]{0:T(1024)} %param.27) | copy-start | bytes 12292
Sparse Core Ops, SparseCore 0:
  8.9 13.2 all-gather.4
  28.3 113.4 all-gather.6
  144.5 110.4 all-gather.8
  442.6 7.7 reduce-scatter.1
where the time goes:
time: 465 us; the launch traced here: 463 us
  waiting for transfers between devices  231 us (50%)
  matrix products  92 us (20%)
  local copies, waits for them, and re-layouts  68.4 us (15%)
  other arithmetic  50.2 us (11%)
  between operations  13.3 us (3%)
    all_gather x1, waiting for transfers between devices, body(): lax.all_gather(values, 'sp', axis=0, tiled=True)  113 us
    all_gather x1, waiting for transfers between devices, body(): lax.all_gather(keys, 'sp', axis=0, tiled=True)  95.9 us
    dot_general x4, matrix products, attend_block(): jnp.einsum('ths,shd->thd', weights.astype(jnp.bfloat16), values, preferre...  43.7 us
    dynamic_slice x12, local copies, waits for them, and re-layouts, attend(): lax.scan(step, state, (keys_blocked, values_blocked, gates_blocked, block...  36.5 us
    reduce_sum x4, other arithmetic, attend_block(): totals = factor * totals + jnp.sum(weights, axis=2)  35.1 us
    dot_general x4, matrix products, attend_block(): jnp.einsum('thd,shd->ths', queries, keys, preferred_element_type=jnp.floa...  30.6 us
    dot_general x4, matrix products, product(): return jnp.dot(scaled, weight, preferred_element_type=jnp.float32)  12.8 us
    all_gather x1, waiting for transfers between devices, body(): part = lax.all_gather(tokens, 'tp', axis=1, tiled=True)  12.8 us
  transfers between devices with their start and end apart: 5, of which 5 were waited for; matrix products, arithmetic and copies ran while one was open for 3% of the time, Pallas kernels for 0%

commit v1 on v0

--- a/solution.py
+++ b/solution.py
@@ -7,6 +7,13 @@
 very_low = -1e30
 epsilon = 1e-06
 key_span = 2048
+
+
+def swapped_in(value, axis, along):
+    size = lax.axis_size(axis)
+    blocks = jnp.stack([value for _ in range(size)])
+    blocks = lax.all_to_all(blocks, axis, split_axis=0, concat_axis=0)
+    return jnp.concatenate(blocks, axis=along)
 
 
 def passed_along(block, axis, distance):
@@ -110,10 +117,7 @@
         jnp.zeros((tok_rows, heads, head_size), jnp.float32),
     )
     carry = state
-    pieces = (
-        lax.all_gather(keys, "sp", axis=0, tiled=True),
-        lax.all_gather(values, "sp", axis=0, tiled=True),
-    )
+    pieces = (lax.all_gather(keys, "sp", axis=0, tiled=True), swapped_in(values, "sp", 0))
     state = lax.cond(
         jnp.int32(0) > last_row,
         lambda: carry,

time: 465 us -> 483 us (1.039)
  waiting for transfers between devices: 231 us -> 272 us
  matrix products: 92 us -> 64.3 us
  other arithmetic: 50.2 us -> 37.9 us
  local copies, waits for them, and re-layouts: 68.4 us -> 77.6 us
  starting transfers between devices: 3.77 us -> 10.7 us
    all_gather x1, waiting for transfers between devices: 95.9 us -> 213 us  [body(): lax.all_gather(keys, 'sp', axis=0, tiled=True)]
    all_gather x1 -> x0, waiting for transfers between devices: 113 us -> none  [body(): lax.all_gather(values, 'sp', axis=0, tiled=True)]
    reduce_scatter x1, waiting for transfers between devices: 7.93 us -> 32.3 us  [body(): lax.psum_scatter((lax.dot_general(attention_out, attended, numbers, prefe...]
    dot_general x4, matrix products: 43.7 us -> 23.3 us  [attend_block(): jnp.einsum('ths,shd->thd', weights.astype(jnp.bfloat16), values, preferre...]
    another operation x1 -> x3, local copies, waits for them, and re-layouts: 0.21 us -> 16.8 us  [the longest x1 12.5 us: attend(): values_blocked = values.reshape(pieces, span, heads, head_size)]
    ppermute x1, waiting for transfers between devices: 0.26 us -> 13.3 us  [passed_along(): return lax.ppermute(block, axis, route)]
    reshape x1 -> x0, local copies, waits for them, and re-layouts: 12.5 us -> none  [attend(): values_blocked = values.reshape(pieces, span, heads, head_size)]
    reduce_sum x4, other arithmetic: 35.1 us -> 22.8 us  [attend_block(): totals = factor * totals + jnp.sum(weights, axis=2)]
  transfers between devices with their start and end apart: 5 -> 5, of which waited for: 5 -> 4; matrix products, arithmetic and copies ran while one was open for 3% -> 3% of each run, Pallas kernels for 0% -> 0%
where the time goes in v1:
time: 483 us; the launch traced here: 481 us
  waiting for transfers between devices  272 us (56%)
  local copies, waits for them, and re-layouts  77.6 us (16%)
  matrix products  64.3 us (13%)
  other arithmetic  37.9 us (8%)
  between operations  13.3 us (3%)
  starting transfers between devices  10.7 us (2%)
    all_gather x1, waiting for transfers between devices, body(): lax.all_gather(keys, 'sp', axis=0, tiled=True)  213 us
    dynamic_slice x12, local copies, waits for them, and re-layouts, attend(): lax.scan(step, state, (keys_blocked, values_blocked, gates_blocked, block...  37.8 us
    reduce_scatter x1, waiting for transfers between devices, body(): lax.psum_scatter((lax.dot_general(attention_out, attended, numbers, prefe...  32.3 us
    dot_general x4, matrix products, attend_block(): jnp.einsum('thd,shd->ths', queries, keys, preferred_element_type=jnp.floa...  24.1 us
    dot_general x4, matrix products, attend_block(): jnp.einsum('ths,shd->thd', weights.astype(jnp.bfloat16), values, preferre...  23.3 us
    reduce_sum x4, other arithmetic, attend_block(): totals = factor * totals + jnp.sum(weights, axis=2)  22.8 us
    ppermute x1, waiting for transfers between devices, passed_along(): return lax.ppermute(block, axis, route)  13.3 us
    all_gather x1, waiting for transfers between devices, body(): part = lax.all_gather(tokens, 'tp', axis=1, tiled=True)  12.8 us
  transfers between devices with their start and end apart: 5, of which 4 were waited for; matrix products, arithmetic and copies ran while one was open for 3% of the time, Pallas kernels for 0%

profile of v1, /device:TPU:0, one launch (start us, length us, event | category | flops | bytes accessed | tf_op | source)
XLA Modules:
  0.0 480.8 jit_solution(10107909684643783107)
XLA Ops:
  9.4 12.8 %all-gather.4.cloned.1.call-done = bf16[512,2048]{1,0:T(8,128)(2,1)} async-done(((bf16[512,1024]{1,0:T(8,128)(2,1)}), bf16[512,2048]{1,0:T(8,128)(2,1)}) %all-gather.4.cloned.1.call-update) | async-done | bytes 2097168 | tf_op jit(solution)/shard_map/all_gather | solution.py:98
  24.5 3.7 fusion.34
  31.6 4.0 stack.2
  35.7 6.8 %all-to-all-start = ((bf16[16,512,512]{2,1,0:T(8,128)(2,1)}), bf16[16,512,512]{2,1,0:T(8,128)(2,1)}, u32[]{:S(2)}, u32[]{:S(2)}) async-start(bf16[16,512,512]{2,1,0:T(8,128)(2,1)} %stack.2), calls=%async_computation | async-start | bytes 16777216 | tf_op jit(solution)/shard_map/all_to_all | solution.py:15
  47.6 3.8 collective-permute-start
  52.7 13.3 %collective-permute-done = bf16[15,512]{1,0:T(8,128)(2,1)S(1)} collective-permute-done((bf16[15,512]{1,0:T(8,128)(2,1)S(1)}, bf16[15,512]{1,0:T(8,128)(2,1)S(1)}, u32[]{:S(2)}, u32[]{:S(2)}) %collective-permute-start) | collective-permute-done | bytes 15392 | tf_op jit(solution)/shard_map/ppermute | solution.py:22
  69.2 213.0 %all-gather.6.cloned.1.call-done = bf16[8192,512]{1,0:T(8,128)(2,1)} async-done(((bf16[512,512]{1,0:T(8,128)(2,1)}), bf16[8192,512]{1,0:T(8,128)(2,1)}) %all-gather.6.cloned.1.call-update) | async-done | bytes 8388624 | tf_op jit(solution)/shard_map/all_gather | solution.py:120
  282.1 147.5 %conditional.1 = (f32[512,4]{0,1:T(4,128)S(1)}, f32[512,4,128]{0,2,1:T(8,128)}) conditional(s32[]{:T(128)} %convert_element_type.58, (bf16[8192,512]{1,0:T(8,128)(2,1)}, bf16[16,512,512]{2,1,0:T(8,128)(2,1)}, f32[4,8192]{1,0:T(4,128)}, bf16[512,512]{1,0:T(8,128)(2,1)S(1)}, s32[]{:T(128)}, /*index=5*/f32[512,4]{0,1:T(4,128)}) %tuple.17, () %tuple.18), branch_computations={%region_1.6_spmd, %region_6.7_spmd} | conditional | flops 2229023232 | bytes 126726560 | solution.py:121
  283.3 12.5 %reshape_reshape.2 = bf16[4,2048,4,128]{3,2,1,0:T(4,128)(2,1)} reshape(bf16[16,512,512]{2,1,0:T(8,128)(2,1)} %get-tuple-element.79) | data formatting | bytes 16777216 | tf_op jit(solution)/shard_map/cond/branch_0_fun/reshape;reshape | solution.py:56
  295.9 12.6 %reshape.108 = bf16[4,2048,4,128]{3,2,1,0:T(4,128)(2,1)} reshape(bf16[8192,512]{1,0:T(8,128)(2,1)} %get-tuple-element.75) | data formatting | bytes 16777216 | tf_op jit(solution)/shard_map/cond/branch_0_fun/reshape | solution.py:55
  308.5 121.2 %while.14 = (s32[]{:T(128)}, f32[512,4]{0,1:T(4,128)S(1)}, f32[512,4]{0,1:T(4,128)S(1)}, f32[512,4,128]{0,2,1:T(8,128)}, s32[]{:T(128)}, /*index=5*/s32[4]{0:T(1...) while((s32[]{:T(128)}, f32[512,4]{0,1:T(4,128)S(1)}, ...), condition=%wide.region_5.5_spmd.clone, body=%wide.region_2.4_spmd.clone.sunk | while | flops 2229023232 | bytes 91042040 | solution.py:68
  311.4 4.4 constant_dynamic-slice_fusion.3
  315.8 4.3 copy.46
  320.1 6.0 %fusion.87 = (f32[512,4]{0,1:T(4,128)S(1)}, f32[4,2048,512]{2,1,0:T(8,128)S(1)}) fusion(f32[4,2048]{1,0:T(4,128)S(1)} %dynamic-slice_bitcast_fusion.3, f32[512,4]{0,1:T(4,128)S(1)} %get-tuple-element.303, pred[512,2048]{0,1:T(8,128)(4,1)S(1)} %broadcast_compare_fusion.6, bf16[512,4,128]{2,0,1:T(8,128)(2,1)} %get-tuple-element.302, ...), kind=kOutput, calls=%fused_computation.6.clone.1 | convolution fusion | flops 1094711296 | bytes 20496384 | tf_op jit(solution)/shard_map/cond/branch_0_fun/while/body/eval_jaxpr/thd,shd->ths/dot_general | solution.py:28
  326.2 5.7 %fusion.88 = f32[512,4]{0,1:T(4,128)S(1)} fusion(f32[4,2048,512]{2,1,0:T(8,128)S(1)} %get-tuple-element.265, f32[512,4]{0,1:T(4,128)S(1)} %select_maximum_fusion.2, f32[4,2048]{1,0:T(4,128)S(1)} %dynamic-slice_bitcast_fusion.3, f32[512,4]{0,1:T(4,128)S(1)} %get-tuple-element.303, pred[512,2048]{0,1:T(8,128)(4,1)S(1)} %broadcast_compare_fusion.6), kind=kLoop, calls=%fused_computation.5.clone.1 | loop fusion | flops 29358080 | bytes 17883136 | tf_op jit(solution)/shard_map/cond/branch_0_fun/while/body/eval_jaxpr/reduce_sum | solution.py:39
  331.9 5.8 %fusion.90 = f32[512,4,128]{0,2,1:T(8,128)S(1)} fusion(f32[4,2048,512]{2,1,0:T(8,128)S(1)} %get-tuple-element.265, f32[512,4]{0,1:T(4,128)S(1)} %select_maximum_fusion.2, f32[4,2048]{1,0:T(4,128)S(1)} %dynamic-slice_bitcast_fusion.3, f32[512,4]{0,1:T(4,128)S(1)} %get-tuple-element.303, pred[512,2048]{0,1:T(8,128)(4,1)S(1)} %broadcast_compare_fusion.6, ...), kind=kOutput, calls=%fused_computation.14.clone.1 | convolution fusion | flops 1103888384 | bytes 22077440 | tf_op jit(solution)/shard_map/cond/branch_0_fun/while/body/eval_jaxpr/ths,shd->thd/dot_general | solution.py:40
  341.6 4.4 constant_dynamic-slice_fusion.3
  346.1 4.3 copy.46
  350.4 6.0 %fusion.87 = (f32[512,4]{0,1:T(4,128)S(1)}, f32[4,2048,512]{2,1,0:T(8,128)S(1)}) fusion(f32[4,2048]{1,0:T(4,128)S(1)} %dynamic-slice_bitcast_fusion.3, f32[512,4]{0,1:T(4,128)S(1)} %get-tuple-element.303, pred[512,2048]{0,1:T(8,128)(4,1)S(1)} %broadcast_compare_fusion.6, bf16[512,4,128]{2,0,1:T(8,128)(2,1)} %get-tuple-element.302, ...), kind=kOutput, calls=%fused_computation.6.clone.1 | convolution fusion | flops 1094711296 | bytes 20496384 | tf_op jit(solution)/shard_map/cond/branch_0_fun/while/body/eval_jaxpr/thd,shd->ths/dot_general | solution.py:28
  356.5 5.7 %fusion.88 = f32[512,4]{0,1:T(4,128)S(1)} fusion(f32[4,2048,512]{2,1,0:T(8,128)S(1)} %get-tuple-element.265, f32[512,4]{0,1:T(4,128)S(1)} %select_maximum_fusion.2, f32[4,2048]{1,0:T(4,128)S(1)} %dynamic-slice_bitcast_fusion.3, f32[512,4]{0,1:T(4,128)S(1)} %get-tuple-element.303, pred[512,2048]{0,1:T(8,128)(4,1)S(1)} %broadcast_compare_fusion.6), kind=kLoop, calls=%fused_computation.5.clone.1 | loop fusion | flops 29358080 | bytes 17883136 | tf_op jit(solution)/shard_map/cond/branch_0_fun/while/body/eval_jaxpr/reduce_sum | solution.py:39
  362.2 5.8 %fusion.90 = f32[512,4,128]{0,2,1:T(8,128)S(1)} fusion(f32[4,2048,512]{2,1,0:T(8,128)S(1)} %get-tuple-element.265, f32[512,4]{0,1:T(4,128)S(1)} %select_maximum_fusion.2, f32[4,2048]{1,0:T(4,128)S(1)} %dynamic-slice_bitcast_fusion.3, f32[512,4]{0,1:T(4,128)S(1)} %get-tuple-element.303, pred[512,2048]{0,1:T(8,128)(4,1)S(1)} %broadcast_compare_fusion.6, ...), kind=kOutput, calls=%fused_computation.14.clone.1 | convolution fusion | flops 1103888384 | bytes 22077440 | tf_op jit(solution)/shard_map/cond/branch_0_fun/while/body/eval_jaxpr/ths,shd->thd/dot_general | solution.py:40
  371.9 4.4 constant_dynamic-slice_fusion.3
  376.4 4.3 copy.46
  380.7 6.0 %fusion.87 = (f32[512,4]{0,1:T(4,128)S(1)}, f32[4,2048,512]{2,1,0:T(8,128)S(1)}) fusion(f32[4,2048]{1,0:T(4,128)S(1)} %dynamic-slice_bitcast_fusion.3, f32[512,4]{0,1:T(4,128)S(1)} %get-tuple-element.303, pred[512,2048]{0,1:T(8,128)(4,1)S(1)} %broadcast_compare_fusion.6, bf16[512,4,128]{2,0,1:T(8,128)(2,1)} %get-tuple-element.302, ...), kind=kOutput, calls=%fused_computation.6.clone.1 | convolution fusion | flops 1094711296 | bytes 20496384 | tf_op jit(solution)/shard_map/cond/branch_0_fun/while/body/eval_jaxpr/thd,shd->ths/dot_general | solution.py:28
  386.8 5.7 %fusion.88 = f32[512,4]{0,1:T(4,128)S(1)} fusion(f32[4,2048,512]{2,1,0:T(8,128)S(1)} %get-tuple-element.265, f32[512,4]{0,1:T(4,128)S(1)} %select_maximum_fusion.2, f32[4,2048]{1,0:T(4,128)S(1)} %dynamic-slice_bitcast_fusion.3, f32[512,4]{0,1:T(4,128)S(1)} %get-tuple-element.303, pred[512,2048]{0,1:T(8,128)(4,1)S(1)} %broadcast_compare_fusion.6), kind=kLoop, calls=%fused_computation.5.clone.1 | loop fusion | flops 29358080 | bytes 17883136 | tf_op jit(solution)/shard_map/cond/branch_0_fun/while/body/eval_jaxpr/reduce_sum | solution.py:39
  392.5 5.8 %fusion.90 = f32[512,4,128]{0,2,1:T(8,128)S(1)} fusion(f32[4,2048,512]{2,1,0:T(8,128)S(1)} %get-tuple-element.265, f32[512,4]{0,1:T(4,128)S(1)} %select_maximum_fusion.2, f32[4,2048]{1,0:T(4,128)S(1)} %dynamic-slice_bitcast_fusion.3, f32[512,4]{0,1:T(4,128)S(1)} %get-tuple-element.303, pred[512,2048]{0,1:T(8,128)(4,1)S(1)} %broadcast_compare_fusion.6, ...), kind=kOutput, calls=%fused_computation.14.clone.1 | convolution fusion | flops 1103888384 | bytes 22077440 | tf_op jit(solution)/shard_map/cond/branch_0_fun/while/body/eval_jaxpr/ths,shd->thd/dot_general | solution.py:40
  402.2 4.4 constant_dynamic-slice_fusion.3
  406.7 4.3 copy.46
  411.0 6.0 %fusion.87 = (f32[512,4]{0,1:T(4,128)S(1)}, f32[4,2048,512]{2,1,0:T(8,128)S(1)}) fusion(f32[4,2048]{1,0:T(4,128)S(1)} %dynamic-slice_bitcast_fusion.3, f32[512,4]{0,1:T(4,128)S(1)} %get-tuple-element.303, pred[512,2048]{0,1:T(8,128)(4,1)S(1)} %broadcast_compare_fusion.6, bf16[512,4,128]{2,0,1:T(8,128)(2,1)} %get-tuple-element.302, ...), kind=kOutput, calls=%fused_computation.6.clone.1 | convolution fusion | flops 1094711296 | bytes 20496384 | tf_op jit(solution)/shard_map/cond/branch_0_fun/while/body/eval_jaxpr/thd,shd->ths/dot_general | solution.py:28
  417.1 5.7 %fusion.88 = f32[512,4]{0,1:T(4,128)S(1)} fusion(f32[4,2048,512]{2,1,0:T(8,128)S(1)} %get-tuple-element.265, f32[512,4]{0,1:T(4,128)S(1)} %select_maximum_fusion.2, f32[4,2048]{1,0:T(4,128)S(1)} %dynamic-slice_bitcast_fusion.3, f32[512,4]{0,1:T(4,128)S(1)} %get-tuple-element.303, pred[512,2048]{0,1:T(8,128)(4,1)S(1)} %broadcast_compare_fusion.6), kind=kLoop, calls=%fused_computation.5.clone.1 | loop fusion | flops 29358080 | bytes 17883136 | tf_op jit(solution)/shard_map/cond/branch_0_fun/while/body/eval_jaxpr/reduce_sum | solution.py:39
  422.8 5.8 %fusion.90 = f32[512,4,128]{0,2,1:T(8,128)S(1)} fusion(f32[4,2048,512]{2,1,0:T(8,128)S(1)} %get-tuple-element.265, f32[512,4]{0,1:T(4,128)S(1)} %select_maximum_fusion.2, f32[4,2048]{1,0:T(4,128)S(1)} %dynamic-slice_bitcast_fusion.3, f32[512,4]{0,1:T(4,128)S(1)} %get-tuple-element.303, pred[512,2048]{0,1:T(8,128)(4,1)S(1)} %broadcast_compare_fusion.6, ...), kind=kOutput, calls=%fused_computation.14.clone.1 | convolution fusion | flops 1103888384 | bytes 22077440 | tf_op jit(solution)/shard_map/cond/branch_0_fun/while/body/eval_jaxpr/ths,shd->thd/dot_general | solution.py:40
  435.5 32.3 %reduce-scatter.2.cloned.1.call-done = bf16[1024,512]{0,1:T(8,128)(2,1)} async-done(((bf16[2048,512]{0,1:T(8,128)(2,1)}), bf16[1024,512]{0,1:T(8,128)(2,1)}) %reduce-scatter.2.cloned.1.call-update) | async-done | bytes 1048592 | tf_op jit(solution)/shard_map/reduce_scatter | solution.py:154
  (114 shorter events, 47.0 us)
Async XLA Ops:
  6.5 424.5 %copy-start = (bf16[512,2048]{1,0:T(8,128)(2,1)S(1)}, bf16[512,2048]{1,0:T(8,128)(2,1)}, u32[]{:S(2)}) copy-start(bf16[512,2048]{1,0:T(8,128)(2,1)} %param.25) | copy-start | bytes 6291460
  6.5 15.7 %all-gather.4.cloned.1.call-start = ((), (), s32[]{:S(2)}) async-start(), calls=%async_computation.2 | async-start | bytes 3145728 | tf_op jit(solution)/shard_map/all_gather | solution.py:98
  7.3 274.9 %all-gather.6.cloned.1.call-start = ((), (), s32[]{:S(2)}) async-start(), calls=%async_computation.3 | async-start | bytes 8912896 | tf_op jit(solution)/shard_map/all_gather | solution.py:120
  22.2 2.2 copy-start.3
  35.7 246.5 %all-to-all-start = ((bf16[16,512,512]{2,1,0:T(8,128)(2,1)}), bf16[16,512,512]{2,1,0:T(8,128)(2,1)}, u32[]{:S(2)}, u32[]{:S(2)}) async-start(bf16[16,512,512]{2,1,0:T(8,128)(2,1)} %stack.2), calls=%async_computation | async-start | bytes 16777216 | tf_op jit(solution)/shard_map/all_to_all | solution.py:15
  42.5 425.3 %reduce-scatter.2.cloned.1.call-start = ((), (), s32[]{:S(2)}) async-start(), calls=%async_computation.4 | async-start | bytes 3145728 | tf_op jit(solution)/shard_map/reduce_scatter | solution.py:154
  43.9 7.5 %copy-start.4 = (bf16[512,2048]{1,0:T(8,128)(2,1)S(1)}, bf16[512,2048]{1,0:T(8,128)(2,1)}, u32[]{:S(2)}) copy-start(bf16[512,2048]{1,0:T(8,128)(2,1)} %all-gather.4.cloned.1.call-done) | copy-start | bytes 6291460
  43.9 7.5 %copy-start.11 = (bf16[2048,512]{1,0:T(8,128)(2,1)S(1)}, bf16[2048,512]{1,0:T(8,128)(2,1)}, u32[]{:S(2)}) copy-start(bf16[2048,512]{1,0:T(8,128)(2,1)} %param.18) | copy-start | bytes 6291460
  47.6 18.4 %collective-permute-start = (bf16[15,512]{1,0:T(8,128)(2,1)S(1)}, bf16[15,512]{1,0:T(8,128)(2,1)S(1)}, u32[]{:S(2)}, u32[]{:S(2)}) collective-permute-start(bf16[15,512]{1,0:T(8,128)(2,1)S(1)} %slice.45), channel_id=1, source_target_pairs={{0,2},{2,4},{4,6},{6,8},{8,10},{10,12},{12,14},{14,16},{16,18},{18... | collective-permute-start | bytes 46088 | tf_op jit(solution)/shard_map/ppermute | solution.py:22
  66.4 0.9 copy-start.12
  67.3 0.9 copy-start.10
  295.9 12.6 %copy-start.8 = (f32[512,4]{0,1:T(4,128)S(1)}, f32[512,4]{0,1:T(4,128)}, u32[]{:S(2)}) copy-start(f32[512,4]{0,1:T(4,128)} %get-tuple-element.277) | copy-start | bytes 24580 | tf_op jit(solution)/shard_map/cond
  326.2 5.8 %copy-start.1 = (bf16[1,2048,4,128]{1,3,2,0:T(8,128)(2,1)S(1)}, bf16[1,2048,4,128]{1,3,2,0:T(8,128)(2,1)}, u32[]{:S(2)}) copy-start(bf16[1,2048,4,128]{1,3,2,0:T(8,128)(2,1)} %copy.46) | copy-start | bytes 6291460 | tf_op jit(solution)/shard_map/cond/branch_0_fun/while
  326.2 5.8 %copy-start.6 = (f32[512,4,128]{0,2,1:T(8,128)S(1)}, f32[512,4,128]{0,2,1:T(8,128)}, u32[]{:S(2)}) copy-start(f32[512,4,128]{0,2,1:T(8,128)} %get-tuple-element.285) | copy-start | bytes 3145732 | tf_op jit(solution)/shard_map/cond/branch_0_fun/while
  337.8 1.0 copy-start.7
  356.5 5.8 %copy-start.1 = (bf16[1,2048,4,128]{1,3,2,0:T(8,128)(2,1)S(1)}, bf16[1,2048,4,128]{1,3,2,0:T(8,128)(2,1)}, u32[]{:S(2)}) copy-start(bf16[1,2048,4,128]{1,3,2,0:T(8,128)(2,1)} %copy.46) | copy-start | bytes 6291460 | tf_op jit(solution)/shard_map/cond/branch_0_fun/while
  356.5 5.8 %copy-start.6 = (f32[512,4,128]{0,2,1:T(8,128)S(1)}, f32[512,4,128]{0,2,1:T(8,128)}, u32[]{:S(2)}) copy-start(f32[512,4,128]{0,2,1:T(8,128)} %get-tuple-element.285) | copy-start | bytes 3145732 | tf_op jit(solution)/shard_map/cond/branch_0_fun/while
  368.1 1.0 copy-start.7
  386.8 5.8 %copy-start.1 = (bf16[1,2048,4,128]{1,3,2,0:T(8,128)(2,1)S(1)}, bf16[1,2048,4,128]{1,3,2,0:T(8,128)(2,1)}, u32[]{:S(2)}) copy-start(bf16[1,2048,4,128]{1,3,2,0:T(8,128)(2,1)} %copy.46) | copy-start | bytes 6291460 | tf_op jit(solution)/shard_map/cond/branch_0_fun/while
  386.8 5.8 %copy-start.6 = (f32[512,4,128]{0,2,1:T(8,128)S(1)}, f32[512,4,128]{0,2,1:T(8,128)}, u32[]{:S(2)}) copy-start(f32[512,4,128]{0,2,1:T(8,128)} %get-tuple-element.285) | copy-start | bytes 3145732 | tf_op jit(solution)/shard_map/cond/branch_0_fun/while
  398.4 1.0 copy-start.7
  417.1 5.8 %copy-start.1 = (bf16[1,2048,4,128]{1,3,2,0:T(8,128)(2,1)S(1)}, bf16[1,2048,4,128]{1,3,2,0:T(8,128)(2,1)}, u32[]{:S(2)}) copy-start(bf16[1,2048,4,128]{1,3,2,0:T(8,128)(2,1)} %copy.46) | copy-start | bytes 6291460 | tf_op jit(solution)/shard_map/cond/branch_0_fun/while
  417.1 5.8 %copy-start.6 = (f32[512,4,128]{0,2,1:T(8,128)S(1)}, f32[512,4,128]{0,2,1:T(8,128)}, u32[]{:S(2)}) copy-start(f32[512,4,128]{0,2,1:T(8,128)} %get-tuple-element.285) | copy-start | bytes 3145732 | tf_op jit(solution)/shard_map/cond/branch_0_fun/while
  428.7 1.0 copy-start.7
  431.0 1.3 copy-start.2
  431.0 1.8 copy-start.5
  435.5 36.3 %copy-start.9 = (f32[1024]{0:T(1024)S(1)}, f32[1024]{0:T(1024)}, u32[]{:S(2)}) copy-start(f32[1024]{0:T(1024)} %param.27) | copy-start | bytes 12292
Sparse Core Ops, SparseCore 0:
  8.9 13.2 all-gather.3
  28.3 253.8 all-gather.5
  435.6 32.1 reduce-scatter.1
